TPU v7x, 32 devices: a whole 2x2x4 slice. The times are simulated.
32 devices in a mesh: grp: 2 (over y), ra: 4 (over z), cb: 4 (over x, core).
Axes of the slice: x: 2, y: 2, z: 4, core: 2. Of those that a mesh axis runs over, the one named last changes fastest.
Arguments:
- tokens: bfloat16 [1024, 4096], P('grp', 'ra'), parts along dimension 0, may hold values from -14 to 14
- pre_gain: bfloat16 [2, 4096], P(None, 'ra'), may hold values from 0.099609375 to 1.8984375
- post_gain: bfloat16 [2, 4096], P(None, 'ra'), may hold values from 0.099609375 to 1.8984375
- gate_weight: bfloat16 [2, 4096, 11008], P(None, 'ra', 'cb'), may hold values from -0.09375 to 0.09375
- up_weight: bfloat16 [2, 4096, 11008], P(None, 'ra', 'cb'), may hold values from -0.09375 to 0.09375
- gate_taps: bfloat16 [2, 3, 11008], P(None, None, 'cb'), may hold values from -3 to 3
- up_taps: bfloat16 [2, 3, 11008], P(None, None, 'cb'), may hold values from -3 to 3
- gate_bias: bfloat16 [2, 11008], P(None, 'cb'), may hold values from -3 to 3
- up_bias: bfloat16 [2, 11008], P(None, 'cb'), may hold values from -3 to 3
- down_weight: bfloat16 [2, 11008, 4096], P(None, 'cb', 'ra'), may hold values from -0.07624929 to 0.07624929
Outputs:
- layer_out: bfloat16 [1024, 4096], P('grp', 'ra'), parts along dimension 0
There are 2 independent parts, one for each index of `grp`. A program takes and returns all parts, laid end to end along the dimension named above; an argument that names none is the same for every part. Nothing has to cross between parts.
All inputs are finite; a program needn't handle non-finite values.
Results may differ from a plain program's by a relative error of at most 0.024.
Values may be sent and summed in bfloat16 or wider, within the bound.
A program may use at most 128 MiB of HBM per device.

v0:
```python
import functools

import jax
import jax.numpy as jnp
from jax import lax
from jax.experimental import pallas as pl
from jax.experimental.pallas import tpu as pltpu
from jax.sharding import PartitionSpec as P

LEN = 256
LANES = 128
SKEW = 2

epsilon = 1e-06
residual_scale = 0.5
MESH = pl.DeviceIdType.MESH


def hidden_kernel(
    layer, n, nx, nch, nfull, fl,
    state_ref, pre_ref, post_ref, coef_ref, wg_hbm, wu_hbm, wd_hbm,
    out_ref,
    w, wd, part, hid, acc, normed, scale, branch, pair_out, pair_in, xbuf, fresh, pre_sq, post_sq,
    wsem, wtail, wdsem, part_send, part_recv, hid_send, hid_recv,
    pre_send, pre_recv, post_send, post_recv, x_send, x_recv, pair_send, pair_recv,
):
    z = lax.axis_index("ra")
    k = lax.axis_index("cb")
    core, xi = k % 2, k // 2
    peer = k + 1 - 2 * core
    tokens, dl = state_ref.shape
    half = tokens // 2
    width = dl * n
    tail = fl - nfull * LANES

    def w_copies(j):
        cols = pl.ds(pl.multiple_of(j * LANES, LANES), LANES)
        return (
            pltpu.make_async_copy(
                wg_hbm.at[layer, cols], w.at[j, pl.ds(0, LANES)], wsem.at[0, j]),
            pltpu.make_async_copy(
                wu_hbm.at[layer, cols], w.at[j, pl.ds(LANES, LANES)], wsem.at[1, j]),
        )

    def tail_copies():
        cols = pl.ds(nfull * LANES, tail)
        return (
            pltpu.make_async_copy(
                wg_hbm.at[layer, cols], w.at[nfull, pl.ds(0, tail)], wtail.at[0]),
            pltpu.make_async_copy(
                wu_hbm.at[layer, cols], w.at[nfull, pl.ds(LANES, tail)], wtail.at[1]),
        )

    barrier = pltpu.get_barrier_semaphore()

    @pl.loop(1, n)
    def _(o):
        pl.semaphore_signal(
            barrier, inc=1, device_id={"ra": (z + o) % n}, device_id_type=MESH)

    pl.semaphore_signal(barrier, inc=1, device_id={"cb": peer}, device_id_type=MESH)
    for o in range(1, nx):
        pl.semaphore_signal(
            barrier, inc=1, device_id={"cb": (xi + o) % nx * 2 + core}, device_id_type=MESH)

    @pl.loop(0, nfull)
    def _(j):
        for copy in w_copies(j):
            copy.start()

    if tail:
        for copy in tail_copies():
            copy.start()
    wd_copy = pltpu.make_async_copy(wd_hbm.at[layer], wd.at[pl.ds(0, fl)], wdsem)
    wd_copy.start()

    eye = lax.broadcasted_iota(jnp.int32, (LANES, LANES), 0) == lax.broadcasted_iota(
        jnp.int32, (LANES, LANES), 1)

    def to_row(column):
        return jnp.sum(jnp.where(eye, column, 0.0), axis=0, keepdims=True)

    def to_column(row):
        return jnp.sum(jnp.where(eye, row, 0.0), axis=1, keepdims=True)

    def sq_copy(buf, send, recv, o, slot):
        return pltpu.make_async_remote_copy(
            src_ref=buf.at[slot], dst_ref=buf.at[slot],
            send_sem=send.at[o], recv_sem=recv.at[slot],
            device_id={"ra": (z + o) % n}, device_id_type=MESH)

    def sq_start(buf, send, recv):
        @pl.loop(1, n)
        def _(o):
            sq_copy(buf, send, recv, o, z).start()

    def sq_wait(buf, send, recv):
        @pl.loop(1, n)
        def _(o):
            sq_copy(buf, send, recv, o, (z + o) % n).wait_recv()

    def scale_of(buf, group):
        total = buf[0, group : group + 1, :]
        for slot in range(1, n):
            total = total + buf[slot, group : group + 1, :]
        return to_column(lax.rsqrt(total / width + epsilon))

    pre_sq[z] = jnp.zeros(pre_sq.shape[1:], jnp.float32)
    post_sq[z] = jnp.zeros(post_sq.shape[1:], jnp.float32)
    for group in range(tokens // LANES):
        rows = slice(group * LANES, (group + 1) * LANES)
        wide = state_ref[rows, :].astype(jnp.float32)
        pre_sq[z, group : group + 1, :] = to_row(jnp.sum(wide * wide, axis=1, keepdims=True))
        normed[rows, :] = (wide * pre_ref[...]).astype(normed.dtype)

    if tail:
        for lo in (0, LANES):
            w[nfull, lo + tail : lo + LANES, :] = jnp.zeros((LANES - tail, dl), w.dtype)
        wd[fl:, :] = jnp.zeros((nch * LANES - fl, wd.shape[1]), wd.dtype)
    acc[...] = jnp.zeros_like(acc)

    pl.semaphore_wait(barrier, n - 1 + nx)
    sq_start(pre_sq, pre_send, pre_recv)

    def place(d):
        if d == 0:
            return n - 1 - z, z - 1, z + 1
        return z, z + 1, z - 1

    def part_copy(d, j, target):
        return pltpu.make_async_remote_copy(
            src_ref=part.at[d, j], dst_ref=part.at[d, j],
            send_sem=part_send.at[d, j], recv_sem=part_recv.at[d, j],
            device_id={"ra": target}, device_id_type=MESH)

    def hid_copy(d, j, target):
        return pltpu.make_async_remote_copy(
            src_ref=hid.at[d, j], dst_ref=hid.at[d, j],
            send_sem=hid_send.at[d, j], recv_sem=hid_recv.at[d, j],
            device_id={"ra": target}, device_id_type=MESH)

    def conv(values, taps, bias):
        rows = lax.broadcasted_iota(jnp.int32, values.shape, 0) % LEN
        count = len(taps)
        result = taps[count - 1] * values
        for offset in range(1, count):
            moved = jnp.where(rows >= offset, pltpu.roll(values, offset, 0), 0.0)
            result = result + taps[count - 1 - offset] * moved
        return result + bias

    def add_down(d, j):
        rows = slice(d * half, (d + 1) * half)
        wrows = pl.ds(pl.multiple_of(j * LANES, LANES), LANES)
        acc[rows, :] += jnp.dot(hid[d, j], wd[wrows, :], preferred_element_type=jnp.float32)

    @pl.loop(0, nch + 2 * (n - 1) * SKEW)
    def _(s):
        @pl.when(s < nfull)
        def _():
            for copy in w_copies(s):
                copy.wait()

        @pl.when(s == 1)
        def _():
            wd_copy.wait()
            if tail:
                for copy in tail_copies():
                    copy.wait()

        @pl.when(s == (n - 1) * SKEW)
        def _():
            sq_wait(pre_sq, pre_send, pre_recv)
            for group in range(tokens // LANES):
                scale[group * LANES : (group + 1) * LANES, :] = scale_of(pre_sq, group)

        for d in range(2):
            p, nxt, prv = place(d)
            rows = slice(d * half, (d + 1) * half)
            c = s - p * SKEW

            @pl.when((c >= 0) & (c < nch))
            def _():
                own = lax.dot_general(
                    normed[rows, :], w[c], (((1,), (1,)), ((), ())),
                    preferred_element_type=jnp.float32)

                @pl.when(p == 0)
                def _():
                    part[d, c] = own.astype(part.dtype)
                    part_copy(d, c, nxt).start()

                @pl.when((p > 0) & (p < n - 1))
                def _():
                    part_copy(d, c, nxt).wait_recv()
                    part[d, c] = (part[d, c].astype(jnp.float32) + own).astype(part.dtype)
                    part_copy(d, c, nxt).start()

                @pl.when(p == n - 1)
                def _():
                    part_copy(d, c, prv).wait_recv()
                    total = (part[d, c].astype(jnp.float32) + own) * scale[rows, :]
                    coef = coef_ref[:, pl.ds(pl.multiple_of(c * LANES, LANES), LANES)]
                    m = coef.shape[0] // 2
                    row = [coef[i : i + 1, :] for i in range(2 * m)]
                    gate = conv(total[:, :LANES], row[: m - 1], row[m - 1])
                    up = conv(total[:, LANES:], row[m : 2 * m - 1], row[2 * m - 1])
                    hid[d, c] = (jax.nn.gelu(gate, approximate=True) * up).astype(hid.dtype)
                    hid_copy(d, c, prv).start()
                    add_down(d, c)

            e = s - (2 * (n - 1) - p) * SKEW

            @pl.when((p < n - 1) & (e >= 0) & (e < nch))
            def _():
                hid_copy(d, e, nxt).wait_recv()

                @pl.when(p > 0)
                def _():
                    hid_copy(d, e, prv).start()

                add_down(d, e)

    kept = pl.ds(pl.multiple_of(core * half, half), half)
    given = pl.ds(pl.multiple_of((1 - core) * half, half), half)
    pair_copy = pltpu.make_async_remote_copy(
        src_ref=pair_out, dst_ref=pair_in,
        send_sem=pair_send.at[0], recv_sem=pair_recv.at[0],
        device_id={"cb": peer}, device_id_type=MESH)
    pair_out[...] = acc[given, :].astype(pair_out.dtype)
    pair_copy.start()
    pair_copy.wait_recv()
    xbuf[xi] = (acc[kept, :] + pair_in[...].astype(jnp.float32)).astype(xbuf.dtype)

    def x_copy(o, slot):
        return pltpu.make_async_remote_copy(
            src_ref=xbuf.at[slot], dst_ref=xbuf.at[slot],
            send_sem=x_send.at[o], recv_sem=x_recv.at[slot],
            device_id={"cb": (xi + o) % nx * 2 + core}, device_id_type=MESH)

    for o in range(1, nx):
        x_copy(o, xi).start()
    for o in range(1, nx):
        x_copy(o, (xi + o) % nx).wait_recv()
    for group in range(half // LANES):
        rows = slice(group * LANES, (group + 1) * LANES)
        total = xbuf[0, rows, :].astype(jnp.float32)
        for i in range(1, nx):
            total = total + xbuf[i, rows, :].astype(jnp.float32)
        branch[rows, :] = total
        post_sq[z, group : group + 1, :] = to_row(jnp.sum(total * total, axis=1, keepdims=True))
    sq_start(post_sq, post_send, post_recv)
    sq_wait(post_sq, post_send, post_recv)
    for group in range(half // LANES):
        rows = slice(group * LANES, (group + 1) * LANES)
        own = pl.ds(pl.multiple_of(core * half + group * LANES, LANES), LANES)
        fresh[own, :] = (
            residual_scale * state_ref[own, :].astype(jnp.float32)
            + branch[rows, :] * scale_of(post_sq, group) * post_ref[...]
        ).astype(fresh.dtype)

    state_copy = pltpu.make_async_remote_copy(
        src_ref=fresh.at[kept], dst_ref=fresh.at[kept],
        send_sem=pair_send.at[1], recv_sem=pair_recv.at[1],
        device_id={"cb": peer}, device_id_type=MESH)
    state_copy.start()
    out_ref[kept, :] = fresh[kept, :]
    pltpu.make_async_remote_copy(
        src_ref=fresh.at[given], dst_ref=fresh.at[given],
        send_sem=pair_send.at[1], recv_sem=pair_recv.at[1],
        device_id={"cb": peer}, device_id_type=MESH).wait_recv()
    out_ref[given, :] = fresh[given, :]

    pair_copy.wait_send()
    state_copy.wait_send()
    for o in range(1, nx):
        x_copy(o, xi).wait_send()

    @pl.loop(1, n)
    def _(o):
        sq_copy(pre_sq, pre_send, pre_recv, o, z).wait_send()
        sq_copy(post_sq, post_send, post_recv, o, z).wait_send()

    for d in range(2):
        p, nxt, prv = place(d)

        @pl.loop(0, nch)
        def _(j):
            @pl.when(p < n - 1)
            def _():
                part_copy(d, j, nxt).wait_send()

            @pl.when(p > 0)
            def _():
                hid_copy(d, j, prv).wait_send()


def sublayer(layer, n, nx, state, pre, post, coef, gate_weight, up_weight, down_weight):
    tokens, dl = state.shape
    fl = gate_weight.shape[1]
    nfull = fl // LANES
    nch = -(-fl // LANES)
    half = tokens // 2
    sq_rows = -(-(tokens // LANES) // 8) * 8
    vmem = pl.BlockSpec(memory_space=pltpu.VMEM)
    hbm = pl.BlockSpec(memory_space=pl.ANY)
    dma = pltpu.SemaphoreType.DMA
    bf16, f32 = jnp.bfloat16, jnp.float32
    return pl.pallas_call(
        functools.partial(hidden_kernel, layer, n, nx, nch, nfull, fl),
        out_shape=jax.ShapeDtypeStruct((tokens, dl), bf16),
        in_specs=[vmem] * 4 + [hbm] * 3,
        out_specs=vmem,
        scratch_shapes=[
            pltpu.VMEM((nch, 2 * LANES, dl), bf16),
            pltpu.VMEM((nch * LANES, dl), bf16),
            pltpu.VMEM((2, nch, half, 2 * LANES), bf16),
            pltpu.VMEM((2, nch, half, LANES), bf16),
            pltpu.VMEM((tokens, dl), f32),
            pltpu.VMEM((tokens, dl), bf16),
            pltpu.VMEM((tokens, 1), f32),
            pltpu.VMEM((half, dl), f32),
            pltpu.VMEM((half, dl), bf16),
            pltpu.VMEM((half, dl), bf16),
            pltpu.VMEM((nx, half, dl), bf16),
            pltpu.VMEM((tokens, dl), bf16),
            pltpu.VMEM((n, sq_rows, LANES), f32),
            pltpu.VMEM((n, sq_rows, LANES), f32),
            dma((2, nch)),
            dma((2,)),
            dma,
            dma((2, nch)),
            dma((2, nch)),
            dma((2, nch)),
            dma((2, nch)),
            dma((n,)),
            dma((n,)),
            dma((n,)),
            dma((n,)),
            dma((nx,)),
            dma((nx,)),
            dma((2,)),
            dma((2,)),
        ],
        compiler_params=pltpu.CompilerParams(
            collective_id=layer, has_side_effects=True, vmem_limit_bytes=56 * 1024 * 1024
        ),
        name=f"hidden_{layer}",
    )(state, pre, post, coef, gate_weight, up_weight, down_weight)


def local(
    n,
    nx,
    tokens,
    pre_gain,
    post_gain,
    gate_weight,
    up_weight,
    gate_taps,
    up_taps,
    gate_bias,
    up_bias,
    down_weight,
):
    padding = -gate_weight.shape[2] % LANES
    coefs = jnp.concatenate(
        [gate_taps, gate_bias[:, None], up_taps, up_bias[:, None]], axis=1
    ).astype(jnp.float32)
    coefs = jnp.pad(coefs, ((0, 0), (0, 0), (0, padding)))
    pre, post = pre_gain.astype(jnp.float32), post_gain.astype(jnp.float32)
    gate_cols = jnp.swapaxes(gate_weight, 1, 2)
    up_cols = jnp.swapaxes(up_weight, 1, 2)
    state = tokens
    for layer in range(gate_weight.shape[0]):
        state = sublayer(
            layer, n, nx, state, pre[layer : layer + 1], post[layer : layer + 1], coefs[layer],
            gate_cols, up_cols, down_weight,
        )
    return state


def solution(mesh):
    in_specs = (
        P("grp", "ra"),
        P(None, "ra"),
        P(None, "ra"),
        P(None, "ra", "cb"),
        P(None, "ra", "cb"),
        P(None, None, "cb"),
        P(None, None, "cb"),
        P(None, "cb"),
        P(None, "cb"),
        P(None, "cb", "ra"),
    )
    body = functools.partial(local, mesh.shape["ra"], mesh.shape["cb"] // 2)
    return jax.shard_map(
        body, mesh=mesh, in_specs=in_specs, out_specs=P("grp", "ra"), check_vma=False
    )
```

profile of v0, /device:TPU:1, one launch (start us, length us, event | category | flops | bytes accessed | tf_op | source)
XLA Modules:
  0.0 283.7 jit_solution(1047870244427706999)
XLA Ops:
  0.0 1.4 fusion.8
  1.4 0.7 copy.14
  2.1 0.7 copy.16
  2.8 0.8 copy.13
  3.6 0.8 copy.15
  4.4 0.1 fusion.7
  4.5 0.7 slice_bitcast_fusion
  5.2 138.8 %hidden_0.1.state_ref = bf16[512,1024]{1,0:T(8,128)(2,1)} custom-call(bf16[512,1024]{1,0:T(8,128)(2,1)} %state_ref.1, f32[1,1024]{1,0:T(1,128)} %get-tuple-element.11.pre_ref, f32[1,1024]{1,0:T(1,128)} %get-tuple-element.8.post_ref, f32[8,2816]{1,0:T(8,128)} %get-tuple-element.6.coef_ref, bf16[2,2752,1024]{2,1,0:T(8,128)(2,1)} %bitcast.8, ...), custom_call_target="tpu_custom_call" | custom-call | tf_op jit(solution)/shard_map/hidden_0/pallas_call | solution.py:308
  144.0 137.5 %hidden_1.1 = bf16[512,1024]{1,0:T(8,128)(2,1)} custom-call(bf16[512,1024]{1,0:T(8,128)(2,1)} %hidden_0.1.state_ref, f32[1,1024]{1,0:T(1,128)} %get-tuple-element.12.pre_ref, f32[1,1024]{1,0:T(1,128)} %get-tuple-element.7.post_ref, f32[8,2816]{1,0:T(8,128)} %get-tuple-element.5.coef_ref, bf16[2,2752,1024]{2,1,0:T(8,128)(2,1)} %bitcast.9, ...), custom_call_target="tpu_custom_call" | custom-call | tf_op jit(solution)/shard_map/hidden_1/pallas_call | solution.py:308
  281.4 2.3 copy.18
where the time goes:
time: 284 us
  Pallas kernels  276 us (97%)
  local copies, waits for them, and re-layouts  7.33 us (3%)
    pallas_call x2, Pallas kernels, sublayer(): pl.pallas_call(functools.partial(hidden_kernel, layer, n, nx, nch, nfull,...  276 us

commit v1 on v0

v1 whole, which is shorter than its diff:
```python
import functools

import jax
import jax.numpy as jnp
from jax import lax
from jax.experimental import pallas as pl
from jax.experimental.pallas import tpu as pltpu
from jax.sharding import PartitionSpec as P

LEN = 256
LANES = 128
BLOCK = 128
HALO = 8
SKEW = 3

epsilon = 1e-06
residual_scale = 0.5
MESH = pl.DeviceIdType.MESH


class Plan:
    def __init__(self, layers, n, nx, tokens, dl, fl):
        self.layers, self.n, self.nx = layers, n, nx
        self.tokens, self.dl, self.fl = tokens, dl, fl
        self.nfull = fl // LANES
        self.nch = -(-fl // LANES)
        self.tail = fl - self.nfull * LANES
        self.blocks = tokens // BLOCK
        self.per_seq = LEN // BLOCK
        self.span = -(-self.nch // 2)
        self.half = BLOCK // 2
        self.stages = layers * self.blocks
        self.turn = (n - 1) * SKEW
        self.done = 2 * self.turn
        self.pair_at = self.done + 1
        self.x_at = self.pair_at + 3
        self.norm_at = self.x_at + 2
        self.next_at = self.norm_at + 1
        self.period = max(
            self.blocks * self.span,
            self.span + self.next_at + 1,
            (self.blocks - 1) * self.span + self.turn + 2,
        )
        self.steps = (layers - 1) * self.period + self.blocks * self.span + self.next_at + 1


def body_kernel(
    plan,
    state_hbm, pre_ref, post_ref, coef_ref, wg_hbm, wu_hbm, wd_hbm,
    out_ref,
    w, wd, part, hid, halo, acc, states, normed, scale, branch, pair_out, pair_in, xbuf, pre_sq, post_sq,
    ssem, wsem, wtail, wdsem, part_send, part_recv, hid_send, hid_recv,
    pre_send, pre_recv, post_send, post_recv, x_send, x_recv, pair_send, pair_recv,
    back_send, back_recv,
):
    z = lax.axis_index("ra")
    k = lax.axis_index("cb")
    core, xi = k % 2, k // 2
    peer = k + 1 - 2 * core
    n, nx, layers, dl, fl = plan.n, plan.nx, plan.layers, plan.dl, plan.fl
    nch, nfull, tail, blocks, span, half = (
        plan.nch, plan.nfull, plan.tail, plan.blocks, plan.span, plan.half)
    width = dl * n
    f32 = jnp.float32

    def w_copies(layer, c):
        cols = pl.ds(pl.multiple_of(c * LANES, LANES), LANES)
        return (
            pltpu.make_async_copy(
                wg_hbm.at[layer, cols], w.at[c, pl.ds(0, LANES)], wsem.at[0, c]),
            pltpu.make_async_copy(
                wu_hbm.at[layer, cols], w.at[c, pl.ds(LANES, LANES)], wsem.at[1, c]),
        )

    def tail_copies(layer):
        cols = pl.ds(nfull * LANES, tail)
        return (
            pltpu.make_async_copy(
                wg_hbm.at[layer, cols], w.at[nfull, pl.ds(0, tail)], wtail.at[0]),
            pltpu.make_async_copy(
                wu_hbm.at[layer, cols], w.at[nfull, pl.ds(LANES, tail)], wtail.at[1]),
        )

    def w_do(layer, c, act):
        @pl.when(c < nfull)
        def _():
            for copy in w_copies(layer, c):
                act(copy)

        if tail:
            @pl.when(c == nfull)
            def _():
                for copy in tail_copies(layer):
                    act(copy)

    def start(copy):
        copy.start()

    def wait(copy):
        copy.wait()

    def wd_copy(layer):
        return pltpu.make_async_copy(
            wd_hbm.at[layer], wd.at[layer, pl.ds(0, fl)], wdsem.at[layer])

    def block_rows(b):
        return pl.ds(pl.multiple_of(b * BLOCK, BLOCK), BLOCK)

    def half_rows(b, which):
        return pl.ds(pl.multiple_of(b * BLOCK + which * half, half), half)

    def state_copy(b):
        return pltpu.make_async_copy(
            state_hbm.at[block_rows(b)], states.at[0, block_rows(b)], ssem.at[b])

    barrier = pltpu.get_barrier_semaphore()

    @pl.loop(1, n)
    def _(o):
        pl.semaphore_signal(
            barrier, inc=1, device_id={"ra": (z + o) % n}, device_id_type=MESH)

    pl.semaphore_signal(barrier, inc=1, device_id={"cb": peer}, device_id_type=MESH)
    for o in range(1, nx):
        pl.semaphore_signal(
            barrier, inc=1, device_id={"cb": (xi + o) % nx * 2 + core}, device_id_type=MESH)

    for b in range(blocks):
        state_copy(b).start()

    @pl.loop(0, nch)
    def _(c):
        w_do(0, c, start)

    for layer in range(layers):
        wd_copy(layer).start()

    def eye(rows):
        shape = (rows, LANES)
        return lax.broadcasted_iota(jnp.int32, shape, 0) == lax.broadcasted_iota(
            jnp.int32, shape, 1)

    def to_row(column):
        return jnp.sum(jnp.where(eye(column.shape[0]), column, 0.0), axis=0, keepdims=True)

    def to_column(row, rows):
        return jnp.sum(jnp.where(eye(rows), row, 0.0), axis=1, keepdims=True)

    def sq_copy(buf, send, recv, t, o, slot):
        return pltpu.make_async_remote_copy(
            src_ref=buf.at[t, slot], dst_ref=buf.at[t, slot],
            send_sem=send.at[t, o], recv_sem=recv.at[t, slot],
            device_id={"ra": (z + o) % n}, device_id_type=MESH)

    def sq_start(buf, send, recv, t):
        @pl.loop(1, n)
        def _(o):
            sq_copy(buf, send, recv, t, o, z).start()

    def sq_wait(buf, send, recv, t):
        @pl.loop(1, n)
        def _(o):
            sq_copy(buf, send, recv, t, o, (z + o) % n).wait_recv()

    def scale_of(buf, t, rows):
        total = buf[t, 0, 0:1, :]
        for slot in range(1, n):
            total = total + buf[t, slot, 0:1, :]
        return to_column(lax.rsqrt(total / width + epsilon), rows)

    def norm(layer, b):
        t = layer * blocks + b
        wide = states[layer, block_rows(b), :].astype(f32)
        normed[block_rows(b), :] = (wide * pre_ref[pl.ds(layer, 1), :]).astype(normed.dtype)
        row = to_row(jnp.sum(wide * wide, axis=1, keepdims=True))
        pre_sq[t, z] = jnp.broadcast_to(row, pre_sq.shape[2:])

    if tail:
        for lo in (0, LANES):
            w[nfull, lo + tail : lo + LANES, :] = jnp.zeros((LANES - tail, dl), w.dtype)
        for layer in range(layers):
            wd[layer, fl:, :] = jnp.zeros((nch * LANES - fl, dl), wd.dtype)

    state_copy(0).wait()
    norm(0, 0)
    pl.semaphore_wait(barrier, n - 1 + nx)
    sq_start(pre_sq, pre_send, pre_recv, 0)

    def place(d):
        if d == 0:
            return n - 1 - z, z - 1, z + 1
        return z, z + 1, z - 1

    def part_copy(d, t, j, target):
        return pltpu.make_async_remote_copy(
            src_ref=part.at[d, t, j], dst_ref=part.at[d, t, j],
            send_sem=part_send.at[d, t, j], recv_sem=part_recv.at[d, t, j],
            device_id={"ra": target}, device_id_type=MESH)

    def hid_copy(d, t, j, target):
        return pltpu.make_async_remote_copy(
            src_ref=hid.at[d, t, j], dst_ref=hid.at[d, t, j],
            send_sem=hid_send.at[d, t, j], recv_sem=hid_recv.at[d, t, j],
            device_id={"ra": target}, device_id_type=MESH)

    def decode(g):
        live = g >= 0
        g = jnp.maximum(g, 0)
        layer = g // plan.period
        rest = g - layer * plan.period
        b = rest // span
        j = rest - b * span
        return live & (layer < layers) & (b < blocks), layer, b, j

    def chunk_of(d, b, j):
        return 2 * j + (d + b // plan.per_seq) % 2

    def conv(values, before, taps, bias):
        rows = lax.broadcasted_iota(jnp.int32, before.shape, 0)
        count = len(taps)
        result = taps[count - 1] * values
        for offset in range(1, count):
            moved = pltpu.roll(values, offset, 0)
            head = jnp.where(rows < offset, pltpu.roll(before, offset, 0), moved[:HALO])
            moved = jnp.concatenate([head, moved[HALO:]], axis=0)
            result = result + taps[count - 1 - offset] * moved
        return result + bias

    def add_down(d, layer, b, j, c):
        wrows = pl.ds(pl.multiple_of(c * LANES, LANES), LANES)
        acc[block_rows(b), :] += jnp.dot(
            hid[d, layer * blocks + b, j], wd[layer, wrows, :], preferred_element_type=f32)

    def pair_copy(t):
        return pltpu.make_async_remote_copy(
            src_ref=pair_out, dst_ref=pair_in.at[t],
            send_sem=pair_send.at[t], recv_sem=pair_recv.at[t],
            device_id={"cb": peer}, device_id_type=MESH)

    def x_copy(t, o, slot):
        return pltpu.make_async_remote_copy(
            src_ref=xbuf.at[t, slot], dst_ref=xbuf.at[t, slot],
            send_sem=x_send.at[t, o], recv_sem=x_recv.at[t, slot],
            device_id={"cb": (xi + o) % nx * 2 + core}, device_id_type=MESH)

    def back_copy(layer, b, which):
        rows = half_rows(b, which)
        t = layer * blocks + b
        return pltpu.make_async_remote_copy(
            src_ref=states.at[layer + 1, rows], dst_ref=states.at[layer + 1, rows],
            send_sem=back_send.at[t], recv_sem=back_recv.at[t],
            device_id={"cb": peer}, device_id_type=MESH)

    @pl.loop(0, plan.steps)
    def _(s):
        @pl.when((s >= 1) & (s < blocks))
        def _():
            state_copy(s).wait()
            norm(0, s)
            sq_start(pre_sq, pre_send, pre_recv, s)

        live, layer, b, j = decode(s - plan.turn)

        @pl.when(live & (j == 0))
        def _():
            t = layer * blocks + b

            @pl.when(b == 0)
            def _():
                wd_copy(layer).wait()

            sq_wait(pre_sq, pre_send, pre_recv, t)
            scale[block_rows(b), :] = scale_of(pre_sq, t, BLOCK)
            acc[block_rows(b), :] = jnp.zeros((BLOCK, dl), f32)

        for d in range(2):
            p, nxt, prv = place(d)
            live, layer, b, j = decode(s - p * SKEW)
            c = chunk_of(d, b, j)
            t = layer * blocks + b

            @pl.when(live & (c < nch))
            def _():
                @pl.when(b == 0)
                def _():
                    w_do(layer, c, wait)

                own = lax.dot_general(
                    normed[block_rows(b), :], w[c], (((1,), (1,)), ((), ())),
                    preferred_element_type=f32)

                @pl.when(p == 0)
                def _():
                    part[d, t, j, 0] = own[:, :LANES].astype(part.dtype)
                    part[d, t, j, 1] = own[:, LANES:].astype(part.dtype)
                    part_copy(d, t, j, nxt).start()

                @pl.when((p > 0) & (p < n - 1))
                def _():
                    part_copy(d, t, j, nxt).wait_recv()
                    for i in range(2):
                        mine = own[:, i * LANES : (i + 1) * LANES]
                        part[d, t, j, i] = (part[d, t, j, i].astype(f32) + mine).astype(part.dtype)
                    part_copy(d, t, j, nxt).start()

                @pl.when(p == n - 1)
                def _():
                    part_copy(d, t, j, prv).wait_recv()
                    coef = coef_ref[layer, :, pl.ds(pl.multiple_of(c * LANES, LANES), LANES)]
                    m = coef.shape[0] // 2
                    row = [coef[i : i + 1, :] for i in range(2 * m)]
                    first = b % plan.per_seq == 0
                    sides = []
                    for i in range(2):
                        mine = own[:, i * LANES : (i + 1) * LANES]
                        total = (part[d, t, j, i].astype(f32) + mine) * scale[block_rows(b), :]
                        before = jnp.where(first, 0.0, halo[d, j, i])
                        halo[d, j, i] = total[BLOCK - HALO :, :]
                        sides.append(
                            conv(total, before, row[i * m : i * m + m - 1], row[i * m + m - 1]))
                    gate, up = sides
                    hid[d, t, j] = (jax.nn.gelu(gate, approximate=True) * up).astype(hid.dtype)
                    hid_copy(d, t, j, prv).start()
                    add_down(d, layer, b, j, c)

                @pl.when((b == blocks - 1) & (layer + 1 < layers))
                def _():
                    w_do(layer + 1, c, start)

        for d in range(2):
            p, nxt, prv = place(d)
            live, layer, b, j = decode(s - (plan.done - p * SKEW))
            c = chunk_of(d, b, j)
            t = layer * blocks + b

            @pl.when(live & (p < n - 1) & (c < nch))
            def _():
                hid_copy(d, t, j, nxt).wait_recv()

                @pl.when(p > 0)
                def _():
                    hid_copy(d, t, j, prv).start()

                add_down(d, layer, b, j, c)

        live, layer, b, j = decode(s - plan.done)

        @pl.when(live & (j == span - 1))
        def _():
            t = layer * blocks + b
            pair_out[...] = acc[half_rows(b, 1 - core), :].astype(pair_out.dtype)
            pair_copy(t).start()

        live, layer, b, j = decode(s - plan.pair_at)

        @pl.when(live & (j == span - 1))
        def _():
            t = layer * blocks + b
            pair_copy(t).wait()
            xbuf[t, xi] = (
                acc[half_rows(b, core), :] + pair_in[t].astype(f32)).astype(xbuf.dtype)
            for o in range(1, nx):
                x_copy(t, o, xi).start()

        live, layer, b, j = decode(s - plan.x_at)

        @pl.when(live & (j == span - 1))
        def _():
            t = layer * blocks + b
            for o in range(1, nx):
                x_copy(t, o, (xi + o) % nx).wait_recv()
            total = xbuf[t, 0].astype(f32)
            for i in range(1, nx):
                total = total + xbuf[t, i].astype(f32)
            branch[...] = total
            row = to_row(jnp.sum(total * total, axis=1, keepdims=True))
            post_sq[t, z] = jnp.broadcast_to(row, post_sq.shape[2:])
            sq_start(post_sq, post_send, post_recv, t)

        live, layer, b, j = decode(s - plan.norm_at)

        @pl.when(live & (j == span - 1))
        def _():
            t = layer * blocks + b
            sq_wait(post_sq, post_send, post_recv, t)
            rows = half_rows(b, core)
            states[layer + 1, rows, :] = (
                residual_scale * states[layer, rows, :].astype(f32)
                + branch[...] * scale_of(post_sq, t, half) * post_ref[pl.ds(layer, 1), :]
            ).astype(states.dtype)
            back_copy(layer, b, core).start()

        live, layer, b, j = decode(s - plan.next_at)

        @pl.when(live & (j == span - 1))
        def _():
            t = layer * blocks + b
            back_copy(layer, b, 1 - core).wait_recv()

            @pl.when(layer + 1 < layers)
            def _():
                norm(layer + 1, b)
                sq_start(pre_sq, pre_send, pre_recv, t + blocks)

            @pl.when(layer + 1 == layers)
            def _():
                out_ref[block_rows(b), :] = states[layers, block_rows(b), :]

    @pl.loop(0, plan.stages)
    def _(t):
        layer = t // blocks
        back_copy(layer, t - layer * blocks, core).wait_send()
        for o in range(1, nx):
            x_copy(t, o, xi).wait_send()

        @pl.loop(1, n)
        def _(o):
            sq_copy(pre_sq, pre_send, pre_recv, t, o, z).wait_send()
            sq_copy(post_sq, post_send, post_recv, t, o, z).wait_send()

        for d in range(2):
            p, nxt, prv = place(d)

            @pl.loop(0, span)
            def _(j):
                b = t - layer * blocks

                @pl.when(chunk_of(d, b, j) < nch)
                def _():
                    @pl.when(p < n - 1)
                    def _():
                        part_copy(d, t, j, nxt).wait_send()

                    @pl.when(p > 0)
                    def _():
                        hid_copy(d, t, j, prv).wait_send()


def run(plan, state, pre, post, coef, gate_weight, up_weight, down_weight):
    vmem = pl.BlockSpec(memory_space=pltpu.VMEM)
    hbm = pl.BlockSpec(memory_space=pl.ANY)
    dma = pltpu.SemaphoreType.DMA
    bf16, f32 = jnp.bfloat16, jnp.float32
    n, nx, dl, nch, span, stages = plan.n, plan.nx, plan.dl, plan.nch, plan.span, plan.stages
    return pl.pallas_call(
        functools.partial(body_kernel, plan),
        out_shape=jax.ShapeDtypeStruct((plan.tokens, dl), bf16),
        in_specs=[hbm, vmem, vmem, vmem, hbm, hbm, hbm],
        out_specs=vmem,
        scratch_shapes=[
            pltpu.VMEM((nch, 2 * LANES, dl), bf16),
            pltpu.VMEM((plan.layers, nch * LANES, dl), bf16),
            pltpu.VMEM((2, stages, span, 2, BLOCK, LANES), bf16),
            pltpu.VMEM((2, stages, span, BLOCK, LANES), bf16),
            pltpu.VMEM((2, span, 2, HALO, LANES), f32),
            pltpu.VMEM((plan.tokens, dl), f32),
            pltpu.VMEM((plan.layers + 1, plan.tokens, dl), bf16),
            pltpu.VMEM((plan.tokens, dl), bf16),
            pltpu.VMEM((plan.tokens, 1), f32),
            pltpu.VMEM((plan.half, dl), f32),
            pltpu.VMEM((plan.half, dl), bf16),
            pltpu.VMEM((stages, plan.half, dl), bf16),
            pltpu.VMEM((stages, nx, plan.half, dl), bf16),
            pltpu.VMEM((stages, n, 8, LANES), f32),
            pltpu.VMEM((stages, n, 8, LANES), f32),
            dma((plan.blocks,)),
            dma((2, nch)),
            dma((2,)),
            dma((plan.layers,)),
            dma((2, stages, span)),
            dma((2, stages, span)),
            dma((2, stages, span)),
            dma((2, stages, span)),
            dma((stages, n)),
            dma((stages, n)),
            dma((stages, n)),
            dma((stages, n)),
            dma((stages, nx)),
            dma((stages, nx)),
            dma((stages,)),
            dma((stages,)),
            dma((stages,)),
            dma((stages,)),
        ],
        compiler_params=pltpu.CompilerParams(
            collective_id=0, has_side_effects=True, vmem_limit_bytes=58 * 1024 * 1024
        ),
        name="sublayers",
    )(state, pre, post, coef, gate_weight, up_weight, down_weight)


def local(
    n,
    nx,
    tokens,
    pre_gain,
    post_gain,
    gate_weight,
    up_weight,
    gate_taps,
    up_taps,
    gate_bias,
    up_bias,
    down_weight,
):
    layers, dl, fl = gate_weight.shape
    plan = Plan(layers, n, nx, tokens.shape[0], dl, fl)
    padding = -fl % LANES
    coefs = jnp.concatenate(
        [gate_taps, gate_bias[:, None], up_taps, up_bias[:, None]], axis=1
    ).astype(jnp.float32)
    coefs = jnp.pad(coefs, ((0, 0), (0, 0), (0, padding)))
    pre, post = pre_gain.astype(jnp.float32), post_gain.astype(jnp.float32)
    gate_cols = jnp.swapaxes(gate_weight, 1, 2)
    up_cols = jnp.swapaxes(up_weight, 1, 2)
    return run(plan, tokens, pre, post, coefs, gate_cols, up_cols, down_weight)


def solution(mesh):
    in_specs = (
        P("grp", "ra"),
        P(None, "ra"),
        P(None, "ra"),
        P(None, "ra", "cb"),
        P(None, "ra", "cb"),
        P(None, None, "cb"),
        P(None, None, "cb"),
        P(None, "cb"),
        P(None, "cb"),
        P(None, "cb", "ra"),
    )
    body = functools.partial(local, mesh.shape["ra"], mesh.shape["cb"] // 2)
    return jax.shard_map(
        body, mesh=mesh, in_specs=in_specs, out_specs=P("grp", "ra"), check_vma=False
    )
```

time: 284 us -> 246 us (0.87)
  Pallas kernels: 276 us -> 237 us
  other arithmetic: 0.11 us -> 3.35 us
    pallas_call x2 -> x1, Pallas kernels: 276 us -> 237 us  [run(): pl.pallas_call(functools.partial(body_kernel, plan), out_shape=jax.ShapeD...]
where the time goes in v1:
time: 246 us; the launch traced here: 245 us
  Pallas kernels  237 us (96%)
  local copies, waits for them, and re-layouts  5.27 us (2%)
  other arithmetic  3.35 us (1%)
    pallas_call x1, Pallas kernels, run(): pl.pallas_call(functools.partial(body_kernel, plan), out_shape=jax.ShapeD...  237 us

profile of v1, /device:TPU:1, one launch (start us, length us, event | category | flops | bytes accessed | tf_op | source)
XLA Modules:
  0.0 245.5 jit_solution(3724356063847109750)
XLA Ops:
  0.0 1.3 convert_element_type.9.pre_ref
  1.3 1.3 convert_element_type.10.post_ref
  2.6 0.7 copy.14
  3.3 0.7 copy.16
  4.0 0.8 copy.13
  4.8 0.8 copy.15
  5.6 0.8 fusion.7.coef_ref
  6.4 236.8 %sublayers.1 = bf16[512,1024]{1,0:T(8,128)(2,1)} custom-call(bf16[512,1024]{1,0:T(8,128)(2,1)} %state_hbm.1, f32[2,1024]{1,0:T(2,128)} %convert_element_type.9.pre_ref, f32[2,1024]{1,0:T(2,128)} %convert_element_type.10.post_ref, f32[2,8,2816]{2,1,0:T(8,128)} %fusion.7.coef_ref, bf16[2,2752,1024]{2,1,0:T(8,128)(2,1)} %bitcast.4, ...), custom_call_target="tpu_custom_call" | custom-call | tf_op jit(solution)/shard_map/sublayers/pallas_call | solution.py:445
  243.2 2.3 copy.18

commit v2 on v1

v2 whole, which is shorter than its diff:
```python
import functools

import jax
import jax.numpy as jnp
from jax import lax
from jax.experimental import pallas as pl
from jax.experimental.pallas import tpu as pltpu
from jax.sharding import PartitionSpec as P

LEN = 256
LANES = 128
BLOCK = 128
HALO = 8
SUM_SKEW = 3
HID_SKEW = 3

epsilon = 1e-06
residual_scale = 0.5
MESH = pl.DeviceIdType.MESH


class Plan:
    def __init__(self, layers, n, nx, tokens, dl, fl, taps):
        self.layers, self.n, self.nx = layers, n, nx
        self.tokens, self.dl, self.fl = tokens, dl, fl
        self.side = taps + 1
        self.nfull = fl // LANES
        self.nch = -(-fl // LANES)
        self.tail = fl - self.nfull * LANES
        self.packed = 0 < 2 * self.tail <= LANES
        self.blocks = tokens // BLOCK
        self.per_seq = LEN // BLOCK
        self.span = -(-self.nch // 2)
        self.half = BLOCK // 2
        self.stages = layers * self.blocks
        self.tiles = [
            layers * sum(self.tiles_of(d, b) for b in range(self.blocks)) for d in range(2)]
        self.hids = [
            layers * sum(len(self.chunks(d, b)) for b in range(self.blocks)) for d in range(2)]
        self.turn = (n - 1) * SUM_SKEW
        self.done = self.turn + (n - 1) * HID_SKEW
        self.pair_at = self.done + 2
        self.x_at = self.pair_at + 4
        self.norm_at = self.x_at + 3
        self.next_at = self.norm_at + 1
        self.period = max(
            self.blocks * self.span,
            self.span + self.next_at + 1,
            (self.blocks - 1) * self.span + self.turn + 2,
        )
        self.steps = (layers - 1) * self.period + self.blocks * self.span + self.next_at + 1

    def chunks(self, d, b):
        return range((d + b // self.per_seq) % 2, self.nch, 2)

    def tiles_of(self, d, b):
        chunks = self.chunks(d, b)
        return 2 * len(chunks) - (1 if self.packed and self.nfull in chunks else 0)


def body_kernel(
    plan,
    state_hbm, pre_ref, post_ref, gt_ref, ut_ref, gb_ref, ub_ref, wg_hbm, wu_hbm, wd_hbm,
    out_ref,
    gains, coefs, w, wd, part, hid, halo, acc, states, normed, scale, branch, pair_out, pair_in, xbuf, pre_sq, post_sq,
    ssem, wsem, wtail, wdsem, part_send, part_recv, hid_send, hid_recv,
    pre_send, pre_recv, post_send, post_recv, x_send, x_recv, pair_send, pair_recv,
    back_send, back_recv,
):
    z = lax.axis_index("ra")
    k = lax.axis_index("cb")
    core, xi = k % 2, k // 2
    peer = k + 1 - 2 * core
    n, nx, layers, dl, fl = plan.n, plan.nx, plan.layers, plan.dl, plan.fl
    nch, nfull, tail, blocks, span, half = (
        plan.nch, plan.nfull, plan.tail, plan.blocks, plan.span, plan.half)
    width = dl * n
    f32 = jnp.float32

    def w_copies(layer, c):
        cols = pl.ds(pl.multiple_of(c * LANES, LANES), LANES)
        return (
            pltpu.make_async_copy(
                wg_hbm.at[layer, cols], w.at[c, pl.ds(0, LANES)], wsem.at[0, c]),
            pltpu.make_async_copy(
                wu_hbm.at[layer, cols], w.at[c, pl.ds(LANES, LANES)], wsem.at[1, c]),
        )

    up_at = tail if plan.packed else LANES

    def tail_copies(layer):
        cols = pl.ds(nfull * LANES, tail)
        return (
            pltpu.make_async_copy(
                wg_hbm.at[layer, cols], w.at[nfull, pl.ds(0, tail)], wtail.at[0]),
            pltpu.make_async_copy(
                wu_hbm.at[layer, cols], w.at[nfull, pl.ds(up_at, tail)], wtail.at[1]),
        )

    def w_do(layer, c, act):
        @pl.when(c < nfull)
        def _():
            for copy in w_copies(layer, c):
                act(copy)

        if tail:
            @pl.when(c == nfull)
            def _():
                for copy in tail_copies(layer):
                    act(copy)

    def start(copy):
        copy.start()

    def wait(copy):
        copy.wait()

    def wd_copy(layer):
        return pltpu.make_async_copy(
            wd_hbm.at[layer], wd.at[layer, pl.ds(0, fl)], wdsem.at[layer])

    def block_rows(b):
        return pl.ds(pl.multiple_of(b * BLOCK, BLOCK), BLOCK)

    def half_rows(b, which):
        return pl.ds(pl.multiple_of(b * BLOCK + which * half, half), half)

    def state_rows(layer, b):
        return block_rows(layer * blocks + b)

    def state_half(layer, b, which):
        return half_rows(layer * blocks + b, which)

    def state_copy(b):
        return pltpu.make_async_copy(
            state_hbm.at[block_rows(b)], states.at[block_rows(b)], ssem.at[b])

    barrier = pltpu.get_barrier_semaphore()

    @pl.loop(1, n)
    def _(o):
        pl.semaphore_signal(
            barrier, inc=1, device_id={"ra": (z + o) % n}, device_id_type=MESH)

    pl.semaphore_signal(barrier, inc=1, device_id={"cb": peer}, device_id_type=MESH)
    for o in range(1, nx):
        pl.semaphore_signal(
            barrier, inc=1, device_id={"cb": (xi + o) % nx * 2 + core}, device_id_type=MESH)

    for b in range(blocks):
        state_copy(b).start()

    @pl.loop(0, nch)
    def _(c):
        w_do(0, c, start)

    for layer in range(layers):
        wd_copy(layer).start()

    def eye(rows):
        shape = (rows, LANES)
        return lax.broadcasted_iota(jnp.int32, shape, 0) == lax.broadcasted_iota(
            jnp.int32, shape, 1)

    def to_row(column):
        return jnp.sum(jnp.where(eye(column.shape[0]), column, 0.0), axis=0, keepdims=True)

    def to_column(row, rows):
        return jnp.sum(jnp.where(eye(rows), row, 0.0), axis=1, keepdims=True)

    def sq_copy(buf, send, recv, t, o, slot):
        return pltpu.make_async_remote_copy(
            src_ref=buf.at[t * n + slot], dst_ref=buf.at[t * n + slot],
            send_sem=send.at[0], recv_sem=recv.at[t, slot],
            device_id={"ra": (z + o) % n}, device_id_type=MESH)

    def sq_start(buf, send, recv, t):
        @pl.loop(1, n)
        def _(o):
            sq_copy(buf, send, recv, t, o, z).start()

    def sq_wait(buf, send, recv, t):
        @pl.loop(1, n)
        def _(o):
            sq_copy(buf, send, recv, t, o, (z + o) % n).wait_recv()

    def scale_of(buf, t, rows):
        total = buf[t * n, 0:1, :]
        for slot in range(1, n):
            total = total + buf[t * n + slot, 0:1, :]
        return to_column(lax.rsqrt(total / width + epsilon), rows)

    def norm(layer, b):
        t = layer * blocks + b
        wide = states[state_rows(layer, b), :].astype(f32)
        normed[block_rows(b), :] = (wide * gains[layer, 0:1, :]).astype(normed.dtype)
        row = to_row(jnp.sum(wide * wide, axis=1, keepdims=True))
        pre_sq[t * n + z] = jnp.broadcast_to(row, pre_sq.shape[1:])

    if tail:
        for lo, hi in ((tail, up_at), (up_at + tail, 2 * LANES)):
            if lo < hi:
                w[nfull, lo:hi, :] = jnp.zeros((hi - lo, dl), w.dtype)
        for layer in range(layers):
            wd[layer, fl:, :] = jnp.zeros((nch * LANES - fl, dl), wd.dtype)

    taps = gt_ref.shape[0]
    side = taps + 1
    for layer in range(layers):
        gains[layer, 0:1, :] = pre_ref[layer : layer + 1, :].astype(f32)
        gains[layer, 1:2, :] = post_ref[layer : layer + 1, :].astype(f32)
    state_copy(0).wait()
    norm(0, 0)
    pl.semaphore_wait(barrier, n - 1 + nx)
    sq_start(pre_sq, pre_send, pre_recv, 0)

    def fill_coefs():
        if tail:
            coefs[:, :, nfull * LANES :] = jnp.zeros((layers, coefs.shape[1], LANES), f32)
        for at, (tap_ref, bias_ref) in ((0, (gt_ref, gb_ref)), (side, (ut_ref, ub_ref))):
            for i in range(side):
                both = (tap_ref[i] if i < taps else bias_ref[...]).astype(f32)
                for layer in range(layers):
                    coefs[layer, at + i : at + i + 1, 0:fl] = both[layer : layer + 1, :]
        if plan.packed:
            last = slice(nfull * LANES, (nfull + 1) * LANES)
            for layer in range(layers):
                for i in range(side):
                    up = coefs[layer, side + i : side + i + 1, last]
                    coefs[layer, i : i + 1, last] += pltpu.roll(up, tail, 1)

    def place(d):
        if d == 0:
            return n - 1 - z, z - 1, z + 1
        return z, z + 1, z - 1

    def part_tile(t, j, i):
        return (t * span + j) * 2 + i

    def part_do(d, t, j, c, target, act):
        def go(count):
            tiles = pl.ds(part_tile(t, j, 0), count)
            act(pltpu.make_async_remote_copy(
                src_ref=part.at[d, tiles], dst_ref=part.at[d, tiles],
                send_sem=part_send.at[d], recv_sem=part_recv.at[d, t, j],
                device_id={"ra": target}, device_id_type=MESH))

        if plan.packed:
            @pl.when(c < nfull)
            def _():
                go(2)

            @pl.when(c == nfull)
            def _():
                go(1)
        else:
            go(2)

    def wait_recv(copy):
        copy.wait_recv()

    def hid_copy(d, t, j, target):
        return pltpu.make_async_remote_copy(
            src_ref=hid.at[d, t * span + j], dst_ref=hid.at[d, t * span + j],
            send_sem=hid_send.at[d], recv_sem=hid_recv.at[d, t, j],
            device_id={"ra": target}, device_id_type=MESH)

    def decode(g):
        live = g >= 0
        g = jnp.maximum(g, 0)
        layer = g // plan.period
        rest = g - layer * plan.period
        b = rest // span
        j = rest - b * span
        return live & (layer < layers) & (b < blocks), layer, b, j

    def chunk_of(d, b, j):
        return 2 * j + (d + b // plan.per_seq) % 2

    def conv(values, before, taps, bias):
        rows = lax.broadcasted_iota(jnp.int32, before.shape, 0)
        count = len(taps)
        result = taps[count - 1] * values
        for offset in range(1, count):
            moved = pltpu.roll(values, offset, 0)
            head = jnp.where(rows < offset, pltpu.roll(before, offset, 0), moved[:HALO])
            moved = jnp.concatenate([head, moved[HALO:]], axis=0)
            result = result + taps[count - 1 - offset] * moved
        return result + bias

    def wd_rows(c):
        return pl.ds(pl.multiple_of(c * LANES, LANES), LANES)

    def add_down(d, layer, b, j, c):
        at = (layer * blocks + b) * span + j

        @pl.when(j % 2 == 1)
        def _():
            two = jnp.concatenate([hid[d, at - 1], hid[d, at]], axis=1)
            rows = jnp.concatenate([wd[layer, wd_rows(c - 2), :], wd[layer, wd_rows(c), :]], axis=0)
            acc[block_rows(b), :] += jnp.dot(two, rows, preferred_element_type=f32)

        @pl.when((j % 2 == 0) & (c + 2 >= nch))
        def _():
            acc[block_rows(b), :] += jnp.dot(
                hid[d, at], wd[layer, wd_rows(c), :], preferred_element_type=f32)

    def pair_copy(t):
        return pltpu.make_async_remote_copy(
            src_ref=pair_out, dst_ref=pair_in.at[t],
            send_sem=pair_send.at[t], recv_sem=pair_recv.at[t],
            device_id={"cb": peer}, device_id_type=MESH)

    def x_copy(t, o, slot):
        return pltpu.make_async_remote_copy(
            src_ref=xbuf.at[t * nx + slot], dst_ref=xbuf.at[t * nx + slot],
            send_sem=x_send.at[0], recv_sem=x_recv.at[t, slot],
            device_id={"cb": (xi + o) % nx * 2 + core}, device_id_type=MESH)

    def back_copy(layer, b, which):
        rows = state_half(layer + 1, b, which)
        t = layer * blocks + b
        return pltpu.make_async_remote_copy(
            src_ref=states.at[rows], dst_ref=states.at[rows],
            send_sem=back_send.at[0], recv_sem=back_recv.at[t],
            device_id={"cb": peer}, device_id_type=MESH)

    @pl.loop(0, plan.steps)
    def _(s):
        @pl.when(s == 2)
        def _():
            fill_coefs()

        @pl.when((s >= 1) & (s < blocks))
        def _():
            state_copy(s).wait()
            norm(0, s)
            sq_start(pre_sq, pre_send, pre_recv, s)

        live, layer, b, j = decode(s - plan.turn)

        @pl.when(live & (j == 0))
        def _():
            t = layer * blocks + b

            @pl.when(b == 0)
            def _():
                wd_copy(layer).wait()

            sq_wait(pre_sq, pre_send, pre_recv, t)
            scale[block_rows(b), :] = scale_of(pre_sq, t, BLOCK)
            acc[block_rows(b), :] = jnp.zeros((BLOCK, dl), f32)

        for d in range(2):
            p, nxt, prv = place(d)
            live, layer, b, j = decode(s - p * SUM_SKEW)
            c = chunk_of(d, b, j)
            t = layer * blocks + b

            @pl.when(live & (c < nch))
            def _():
                @pl.when(b == 0)
                def _():
                    w_do(layer, c, wait)

                own = lax.dot_general(
                    normed[block_rows(b), :], w[c], (((1,), (1,)), ((), ())),
                    preferred_element_type=f32)

                def mine(i):
                    return own[:, i * LANES : (i + 1) * LANES]

                def tile(i):
                    return part[d, part_tile(t, j, i)].astype(f32)

                @pl.when(p == 0)
                def _():
                    for i in range(2):
                        part[d, part_tile(t, j, i)] = mine(i).astype(part.dtype)
                    part_do(d, t, j, c, nxt, start)

                @pl.when((p > 0) & (p < n - 1))
                def _():
                    part_do(d, t, j, c, nxt, wait_recv)
                    part[d, part_tile(t, j, 0)] = (tile(0) + mine(0)).astype(part.dtype)

                    @pl.when((c < nfull) | (not plan.packed))
                    def _():
                        part[d, part_tile(t, j, 1)] = (tile(1) + mine(1)).astype(part.dtype)

                    part_do(d, t, j, c, nxt, start)

                @pl.when(p == n - 1)
                def _():
                    part_do(d, t, j, c, prv, wait_recv)
                    coef = coefs[layer, :, wd_rows(c)]
                    row = [coef[i : i + 1, :] for i in range(2 * side)]
                    first = b % plan.per_seq == 0
                    last = plan.packed & (c == nfull)
                    sides = []
                    for i in range(2):
                        arrived = jnp.where(last, 0.0, tile(i)) if i and plan.packed else tile(i)
                        total = (arrived + mine(i)) * scale[block_rows(b), :]
                        before = jnp.where(first, 0.0, halo[d, j, i])
                        halo[d, j, i] = total[BLOCK - HALO :, :]
                        at = i * side
                        sides.append(conv(total, before, row[at : at + taps], row[at + taps]))
                    gate, up = sides
                    if plan.packed:
                        up = jnp.where(last, pltpu.roll(gate, LANES - tail, 1), up)
                    value = jax.nn.gelu(gate, approximate=True) * up
                    if plan.packed:
                        lane = lax.broadcasted_iota(jnp.int32, value.shape, 1)
                        value = jnp.where(last & (lane >= tail), 0.0, value)
                    hid[d, t * span + j] = value.astype(hid.dtype)
                    hid_copy(d, t, j, prv).start()

                @pl.when((b == blocks - 1) & (layer + 1 < layers))
                def _():
                    w_do(layer + 1, c, start)

        for d in range(2):
            p, nxt, prv = place(d)
            live, layer, b, j = decode(s - (plan.done - p * HID_SKEW))
            c = chunk_of(d, b, j)
            t = layer * blocks + b

            @pl.when(live & (p < n - 1) & (c < nch))
            def _():
                hid_copy(d, t, j, nxt).wait_recv()

                @pl.when(p > 0)
                def _():
                    hid_copy(d, t, j, prv).start()

        for d in range(2):
            p, nxt, prv = place(d)
            live, layer, b, j = decode(s - (plan.done - p * HID_SKEW))
            c = chunk_of(d, b, j)

            @pl.when(live & (c < nch))
            def _():
                add_down(d, layer, b, j, c)

        live, layer, b, j = decode(s - plan.done)

        @pl.when(live & (j == span - 1))
        def _():
            t = layer * blocks + b
            pair_out[...] = acc[half_rows(b, 1 - core), :].astype(pair_out.dtype)
            pair_copy(t).start()

        live, layer, b, j = decode(s - plan.pair_at)

        @pl.when(live & (j == span - 1))
        def _():
            t = layer * blocks + b
            pair_copy(t).wait()
            xbuf[t * nx + xi] = (
                acc[half_rows(b, core), :] + pair_in[t].astype(f32)).astype(xbuf.dtype)
            for o in range(1, nx):
                x_copy(t, o, xi).start()

        live, layer, b, j = decode(s - plan.x_at)

        @pl.when(live & (j == span - 1))
        def _():
            t = layer * blocks + b
            for o in range(1, nx):
                x_copy(t, o, (xi + o) % nx).wait_recv()
            total = xbuf[t * nx].astype(f32)
            for i in range(1, nx):
                total = total + xbuf[t * nx + i].astype(f32)
            branch[...] = total
            row = to_row(jnp.sum(total * total, axis=1, keepdims=True))
            post_sq[t * n + z] = jnp.broadcast_to(row, post_sq.shape[1:])
            sq_start(post_sq, post_send, post_recv, t)

        live, layer, b, j = decode(s - plan.norm_at)

        @pl.when(live & (j == span - 1))
        def _():
            t = layer * blocks + b
            sq_wait(post_sq, post_send, post_recv, t)
            states[state_half(layer + 1, b, core), :] = (
                residual_scale * states[state_half(layer, b, core), :].astype(f32)
                + branch[...] * scale_of(post_sq, t, half) * gains[layer, 1:2, :]
            ).astype(states.dtype)
            back_copy(layer, b, core).start()

        live, layer, b, j = decode(s - plan.next_at)

        @pl.when(live & (j == span - 1))
        def _():
            t = layer * blocks + b
            back_copy(layer, b, 1 - core).wait_recv()

            @pl.when(layer + 1 < layers)
            def _():
                norm(layer + 1, b)
                sq_start(pre_sq, pre_send, pre_recv, t + blocks)

            @pl.when(layer + 1 == layers)
            def _():
                out_ref[block_rows(b), :] = states[state_rows(layers, b), :]

    def all_sent(buf, count, sem):
        sent = buf.at[pl.ds(0, count)]
        pltpu.make_async_remote_copy(
            src_ref=sent, dst_ref=sent, send_sem=sem, recv_sem=pair_recv.at[0],
            device_id={"cb": peer}, device_id_type=MESH).wait_send()

    all_sent(states, plan.stages * half, back_send.at[0])
    if nx > 1:
        all_sent(xbuf, plan.stages * (nx - 1), x_send.at[0])
    all_sent(pre_sq, plan.stages * (n - 1), pre_send.at[0])
    all_sent(post_sq, plan.stages * (n - 1), post_send.at[0])
    for d in range(2):
        p, nxt, prv = place(d)

        @pl.when(p < n - 1)
        def _():
            all_sent(part.at[d], plan.tiles[d], part_send.at[d])

        @pl.when(p > 0)
        def _():
            all_sent(hid.at[d], plan.hids[d], hid_send.at[d])


def run(plan, *operands):
    vmem = pl.BlockSpec(memory_space=pltpu.VMEM)
    hbm = pl.BlockSpec(memory_space=pl.ANY)
    dma = pltpu.SemaphoreType.DMA
    bf16, f32 = jnp.bfloat16, jnp.float32
    n, nx, dl, nch, span, stages = plan.n, plan.nx, plan.dl, plan.nch, plan.span, plan.stages
    return pl.pallas_call(
        functools.partial(body_kernel, plan),
        out_shape=jax.ShapeDtypeStruct((plan.tokens, dl), bf16),
        in_specs=[hbm] + [vmem] * 6 + [hbm] * 3,
        out_specs=vmem,
        scratch_shapes=[
            pltpu.VMEM((plan.layers, 2, dl), f32),
            pltpu.VMEM((plan.layers, 2 * plan.side, nch * LANES), f32),
            pltpu.VMEM((nch, 2 * LANES, dl), bf16),
            pltpu.VMEM((plan.layers, nch * LANES, dl), bf16),
            pltpu.VMEM((2, stages * span * 2, BLOCK, LANES), bf16),
            pltpu.VMEM((2, stages * span, BLOCK, LANES), bf16),
            pltpu.VMEM((2, span, 2, HALO, LANES), f32),
            pltpu.VMEM((plan.tokens, dl), f32),
            pltpu.VMEM(((plan.layers + 1) * plan.tokens, dl), bf16),
            pltpu.VMEM((plan.tokens, dl), bf16),
            pltpu.VMEM((plan.tokens, 1), f32),
            pltpu.VMEM((plan.half, dl), f32),
            pltpu.VMEM((plan.half, dl), bf16),
            pltpu.VMEM((stages, plan.half, dl), bf16),
            pltpu.VMEM((stages * nx, plan.half, dl), bf16),
            pltpu.VMEM((stages * n, 8, LANES), f32),
            pltpu.VMEM((stages * n, 8, LANES), f32),
            dma((plan.blocks,)),
            dma((2, nch)),
            dma((2,)),
            dma((plan.layers,)),
            dma((2,)),
            dma((2, stages, span)),
            dma((2,)),
            dma((2, stages, span)),
            dma((1,)),
            dma((stages, n)),
            dma((1,)),
            dma((stages, n)),
            dma((1,)),
            dma((stages, nx)),
            dma((stages,)),
            dma((stages,)),
            dma((1,)),
            dma((stages,)),
        ],
        compiler_params=pltpu.CompilerParams(
            collective_id=0, has_side_effects=True, vmem_limit_bytes=58 * 1024 * 1024
        ),
        name="sublayers",
    )(*operands)


def local(
    n,
    nx,
    tokens,
    pre_gain,
    post_gain,
    gate_weight,
    up_weight,
    gate_taps,
    up_taps,
    gate_bias,
    up_bias,
    down_weight,
):
    layers, dl, fl = gate_weight.shape
    plan = Plan(layers, n, nx, tokens.shape[0], dl, fl, gate_taps.shape[1])
    return run(
        plan, tokens, pre_gain, post_gain, jnp.swapaxes(gate_taps, 0, 1), jnp.swapaxes(up_taps, 0, 1),
        gate_bias, up_bias, jnp.swapaxes(gate_weight, 1, 2), jnp.swapaxes(up_weight, 1, 2), down_weight)


def solution(mesh):
    in_specs = (
        P("grp", "ra"),
        P(None, "ra"),
        P(None, "ra"),
        P(None, "ra", "cb"),
        P(None, "ra", "cb"),
        P(None, None, "cb"),
        P(None, None, "cb"),
        P(None, "cb"),
        P(None, "cb"),
        P(None, "cb", "ra"),
    )
    body = functools.partial(local, mesh.shape["ra"], mesh.shape["cb"] // 2)
    return jax.shard_map(
        body, mesh=mesh, in_specs=in_specs, out_specs=P("grp", "ra"), check_vma=False
    )
```

time: 246 us -> 228 us (0.927)
  Pallas kernels: 237 us -> 225 us
  other arithmetic: 3.35 us -> 0 us
  local copies, waits for them, and re-layouts: 5.27 us -> 2.26 us
    pallas_call x1, Pallas kernels: 237 us -> 225 us  [run(): pl.pallas_call(functools.partial(body_kernel, plan), out_shape=jax.ShapeD...]
    convert_element_type x2 -> x0, other arithmetic: 2.57 us -> none  [local(): pre, post = (pre_gain.astype(jnp.float32), post_gain.astype(jnp.float32))]
where the time goes in v2:
time: 228 us; the launch traced here: 227 us
  Pallas kernels  225 us (99%)
    pallas_call x1, Pallas kernels, run(): pl.pallas_call(functools.partial(body_kernel, plan), out_shape=jax.ShapeD...  225 us

profile of v2, /device:TPU:1, one launch (start us, length us, event | category | flops | bytes accessed | tf_op | source)
XLA Modules:
  0.0 227.3 jit_solution(4699657734964849326)
XLA Ops:
  0.0 225.1 %sublayers.1 = bf16[512,1024]{1,0:T(8,128)(2,1)} custom-call(bf16[512,1024]{1,0:T(8,128)(2,1)} %state_hbm.1, bf16[2,1024]{1,0:T(2,128)(2,1)} %pre_ref.1, bf16[2,1024]{1,0:T(2,128)(2,1)} %post_ref.1, bf16[3,2,2752]{2,1,0:T(2,128)(2,1)} %bitcast.6, bf16[3,2,2752]{2,1,0:T(2,128)(2,1)} %bitcast.7, bf16[2,2752]{1,0:T(2,128)(2,1)} %gb_ref.1, ...), custom_call_target="tpu_custom_call" | custom-call | tf_op jit(solution)/shard_map/sublayers/pallas_call | solution.py:536
  225.1 2.3 copy.12

commit v3 on v2

--- a/solution.py
+++ b/solution.py
@@ -13,6 +13,7 @@
 HALO = 8
 SUM_SKEW = 3
 HID_SKEW = 3
+LAST = 3
 
 epsilon = 1e-06
 residual_scale = 0.5
@@ -35,20 +36,21 @@
         self.stages = layers * self.blocks
         self.tiles = [
             layers * sum(self.tiles_of(d, b) for b in range(self.blocks)) for d in range(2)]
+        self.lasts = [
+            sum(c // 2 >= self.span - LAST for c in self.chunks(d, self.blocks - 1)) for d in range(2)]
         self.hids = [
-            layers * sum(len(self.chunks(d, b)) for b in range(self.blocks)) for d in range(2)]
+            layers * sum(len(self.chunks(d, b)) for b in range(self.blocks)) - self.lasts[d]
+            for d in range(2)]
         self.turn = (n - 1) * SUM_SKEW
         self.done = self.turn + (n - 1) * HID_SKEW
         self.pair_at = self.done + 2
-        self.x_at = self.pair_at + 4
+        self.x_at = self.pair_at + 8
         self.norm_at = self.x_at + 3
         self.next_at = self.norm_at + 1
-        self.period = max(
-            self.blocks * self.span,
-            self.span + self.next_at + 1,
-            (self.blocks - 1) * self.span + self.turn + 2,
-        )
-        self.steps = (layers - 1) * self.period + self.blocks * self.span + self.next_at + 1
+        least = max(self.span + self.next_at + 1, (self.blocks - 1) * self.span + self.turn + 2)
+        self.lap = max(self.blocks, -(-least // self.span))
+        self.steps = ((layers - 1) * self.lap + self.blocks) * self.span + self.next_at + 1
+        self.ring = -(-(SUM_SKEW + HID_SKEW + 2) // self.span)
 
     def chunks(self, d, b):
         return range((d + b // self.per_seq) % 2, self.nch, 2)
@@ -63,7 +65,7 @@
     state_hbm, pre_ref, post_ref, gt_ref, ut_ref, gb_ref, ub_ref, wg_hbm, wu_hbm, wd_hbm,
     out_ref,
     gains, coefs, w, wd, part, hid, halo, acc, states, normed, scale, branch, pair_out, pair_in, xbuf, pre_sq, post_sq,
-    ssem, wsem, wtail, wdsem, part_send, part_recv, hid_send, hid_recv,
+    ssem, wsem, wtail, wdsem, part_send, part_recv, hid_send, hid_recv, last_recv,
     pre_send, pre_recv, post_send, post_recv, x_send, x_recv, pair_send, pair_recv,
     back_send, back_recv,
 ):
@@ -171,7 +173,7 @@
     def sq_copy(buf, send, recv, t, o, slot):
         return pltpu.make_async_remote_copy(
             src_ref=buf.at[t * n + slot], dst_ref=buf.at[t * n + slot],
-            send_sem=send.at[0], recv_sem=recv.at[t, slot],
+            send_sem=send.at[0], recv_sem=recv.at[t % blocks, slot],
             device_id={"ra": (z + o) % n}, device_id_type=MESH)
 
     def sq_start(buf, send, recv, t):
@@ -242,7 +244,7 @@
             tiles = pl.ds(part_tile(t, j, 0), count)
             act(pltpu.make_async_remote_copy(
                 src_ref=part.at[d, tiles], dst_ref=part.at[d, tiles],
-                send_sem=part_send.at[d], recv_sem=part_recv.at[d, t, j],
+                send_sem=part_send.at[d], recv_sem=part_recv.at[d, slot_of(t, j)],
                 device_id={"ra": target}, device_id_type=MESH))
 
         if plan.packed:
@@ -262,20 +264,53 @@
     def hid_copy(d, t, j, target):
         return pltpu.make_async_remote_copy(
             src_ref=hid.at[d, t * span + j], dst_ref=hid.at[d, t * span + j],
-            send_sem=hid_send.at[d], recv_sem=hid_recv.at[d, t, j],
+            send_sem=hid_send.at[d], recv_sem=hid_recv.at[d, slot_of(t, j)],
             device_id={"ra": target}, device_id_type=MESH)
 
-    def decode(g):
-        live = g >= 0
-        g = jnp.maximum(g, 0)
-        layer = g // plan.period
-        rest = g - layer * plan.period
-        b = rest // span
-        j = rest - b * span
-        return live & (layer < layers) & (b < blocks), layer, b, j
+    def last_copy(d, t, j, target):
+        return pltpu.make_async_remote_copy(
+            src_ref=hid.at[d, t * span + j], dst_ref=hid.at[d, t * span + j],
+            send_sem=hid_send.at[d], recv_sem=last_recv.at[d, j - (span - LAST)],
+            device_id={"ra": target}, device_id_type=MESH)
+
+    def is_last(layer, b, j):
+        return (layer == layers - 1) & (b == blocks - 1) & (j >= span - LAST)
+
+    def one_of(b, members):
+        return functools.reduce(jnp.logical_or, [b == i for i in members], jnp.bool_(False))
+
+    def odd(b):
+        return one_of(b, [i for i in range(blocks) if i // plan.per_seq % 2])
 
     def chunk_of(d, b, j):
-        return 2 * j + (d + b // plan.per_seq) % 2
+        return 2 * j + jnp.where(odd(b), 1 - d, d)
+
+    def slot_of(t, j):
+        return j if plan.ring == 1 else t % plan.ring * span + j
+
+    def advance(at, moving):
+        layer, b, j = at
+        j = j + jnp.where(moving, 1, 0)
+        turn = j == span
+        b = b + jnp.where(turn, 1, 0)
+        lap = b == plan.lap
+        return (
+            layer + jnp.where(lap, 1, 0), jnp.where(lap, 0, b), jnp.where(turn, 0, j))
+
+    def live_at(at, offset, s):
+        layer, b, j = at
+        live = (s >= offset) & (layer < layers)
+        return live if plan.lap == blocks else live & (b < blocks)
+
+    def ago(at, steps):
+        layer, b, j = at
+        laps = -(-steps // span)
+        b = b - laps
+        over = b < 0
+        layer = jnp.where(over, layer - 1, layer)
+        b = jnp.where(over, b + plan.lap, b)
+        hit = (j == (span - 1 + steps) % span) & (layer >= 0) & (layer < layers)
+        return hit if plan.lap == blocks else hit & (b < blocks), layer, b
 
     def conv(values, before, taps, bias):
         rows = lax.broadcasted_iota(jnp.int32, before.shape, 0)
@@ -308,13 +343,13 @@
     def pair_copy(t):
         return pltpu.make_async_remote_copy(
             src_ref=pair_out, dst_ref=pair_in.at[t],
-            send_sem=pair_send.at[t], recv_sem=pair_recv.at[t],
+            send_sem=pair_send.at[t % 2], recv_sem=pair_recv.at[t % 2],
             device_id={"cb": peer}, device_id_type=MESH)
 
     def x_copy(t, o, slot):
         return pltpu.make_async_remote_copy(
             src_ref=xbuf.at[t * nx + slot], dst_ref=xbuf.at[t * nx + slot],
-            send_sem=x_send.at[0], recv_sem=x_recv.at[t, slot],
+            send_sem=x_send.at[0], recv_sem=x_recv.at[t % 2, slot],
             device_id={"cb": (xi + o) % nx * 2 + core}, device_id_type=MESH)
 
     def back_copy(layer, b, which):
@@ -322,11 +357,18 @@
         t = layer * blocks + b
         return pltpu.make_async_remote_copy(
             src_ref=states.at[rows], dst_ref=states.at[rows],
-            send_sem=back_send.at[0], recv_sem=back_recv.at[t],
+            send_sem=back_send.at[0], recv_sem=back_recv.at[t % 2],
             device_id={"cb": peer}, device_id_type=MESH)
 
-    @pl.loop(0, plan.steps)
-    def _(s):
+    offsets = [plan.turn, plan.done]
+    for d in range(2):
+        p = place(d)[0]
+        offsets += [p * SUM_SKEW, plan.done - p * HID_SKEW]
+
+    def step(s, streams):
+        turn_at, done_at = streams[0], streams[1]
+        sum_at, hid_at = streams[2::2], streams[3::2]
+
         @pl.when(s == 2)
         def _():
             fill_coefs()
@@ -337,9 +379,9 @@
             norm(0, s)
             sq_start(pre_sq, pre_send, pre_recv, s)
 
-        live, layer, b, j = decode(s - plan.turn)
-
-        @pl.when(live & (j == 0))
+        layer, b, j = turn_at
+
+        @pl.when(live_at(turn_at, plan.turn, s) & (j == 0))
         def _():
             t = layer * blocks + b
 
@@ -353,7 +395,8 @@
 
         for d in range(2):
             p, nxt, prv = place(d)
-            live, layer, b, j = decode(s - p * SUM_SKEW)
+            layer, b, j = sum_at[d]
+            live = live_at(sum_at[d], p * SUM_SKEW, s)
             c = chunk_of(d, b, j)
             t = layer * blocks + b
 
@@ -395,7 +438,7 @@
                     part_do(d, t, j, c, prv, wait_recv)
                     coef = coefs[layer, :, wd_rows(c)]
                     row = [coef[i : i + 1, :] for i in range(2 * side)]
-                    first = b % plan.per_seq == 0
+                    first = one_of(b, range(0, blocks, plan.per_seq))
                     last = plan.packed & (c == nfull)
                     sides = []
                     for i in range(2):
@@ -413,7 +456,15 @@
                         lane = lax.broadcasted_iota(jnp.int32, value.shape, 1)
                         value = jnp.where(last & (lane >= tail), 0.0, value)
                     hid[d, t * span + j] = value.astype(hid.dtype)
-                    hid_copy(d, t, j, prv).start()
+
+                    @pl.when(jnp.logical_not(is_last(layer, b, j)))
+                    def _():
+                        hid_copy(d, t, j, prv).start()
+
+                    @pl.when(is_last(layer, b, j))
+                    def _():
+                        for o in range(n - 1, 0, -1):
+                            last_copy(d, t, j, z + o * (prv - z)).start()
 
                 @pl.when((b == blocks - 1) & (layer + 1 < layers))
                 def _():
@@ -421,38 +472,47 @@
 
         for d in range(2):
             p, nxt, prv = place(d)
-            live, layer, b, j = decode(s - (plan.done - p * HID_SKEW))
+            layer, b, j = hid_at[d]
+            live = live_at(hid_at[d], plan.done - p * HID_SKEW, s)
             c = chunk_of(d, b, j)
             t = layer * blocks + b
 
             @pl.when(live & (p < n - 1) & (c < nch))
             def _():
-                hid_copy(d, t, j, nxt).wait_recv()
-
-                @pl.when(p > 0)
+                @pl.when(jnp.logical_not(is_last(layer, b, j)))
                 def _():
-                    hid_copy(d, t, j, prv).start()
+                    hid_copy(d, t, j, nxt).wait_recv()
+
+                    @pl.when(p > 0)
+                    def _():
+                        hid_copy(d, t, j, prv).start()
+
+                @pl.when(is_last(layer, b, j))
+                def _():
+                    last_copy(d, t, j, nxt).wait_recv()
 
         for d in range(2):
             p, nxt, prv = place(d)
-            live, layer, b, j = decode(s - (plan.done - p * HID_SKEW))
+            layer, b, j = hid_at[d]
+            live = live_at(hid_at[d], plan.done - p * HID_SKEW, s)
             c = chunk_of(d, b, j)
 
             @pl.when(live & (c < nch))
             def _():
                 add_down(d, layer, b, j, c)
 
-        live, layer, b, j = decode(s - plan.done)
-
-        @pl.when(live & (j == span - 1))
+        started = s >= plan.done
+        hit, layer, b = ago(done_at, 0)
+
+        @pl.when(started & hit)
         def _():
             t = layer * blocks + b
             pair_out[...] = acc[half_rows(b, 1 - core), :].astype(pair_out.dtype)
             pair_copy(t).start()
 
-        live, layer, b, j = decode(s - plan.pair_at)
-
-        @pl.when(live & (j == span - 1))
+        hit, layer, b = ago(done_at, plan.pair_at - plan.done)
+
+        @pl.when(started & hit)
         def _():
             t = layer * blocks + b
             pair_copy(t).wait()
@@ -461,9 +521,9 @@
             for o in range(1, nx):
                 x_copy(t, o, xi).start()
 
-        live, layer, b, j = decode(s - plan.x_at)
-
-        @pl.when(live & (j == span - 1))
+        hit, layer, b = ago(done_at, plan.x_at - plan.done)
+
+        @pl.when(started & hit)
         def _():
             t = layer * blocks + b
             for o in range(1, nx):
@@ -476,9 +536,9 @@
             post_sq[t * n + z] = jnp.broadcast_to(row, post_sq.shape[1:])
             sq_start(post_sq, post_send, post_recv, t)
 
-        live, layer, b, j = decode(s - plan.norm_at)
-
-        @pl.when(live & (j == span - 1))
+        hit, layer, b = ago(done_at, plan.norm_at - plan.done)
+
+        @pl.when(started & hit)
         def _():
             t = layer * blocks + b
             sq_wait(post_sq, post_send, post_recv, t)
@@ -488,9 +548,9 @@
             ).astype(states.dtype)
             back_copy(layer, b, core).start()
 
-        live, layer, b, j = decode(s - plan.next_at)
-
-        @pl.when(live & (j == span - 1))
+        hit, layer, b = ago(done_at, plan.next_at - plan.done)
+
+        @pl.when(started & hit)
         def _():
             t = layer * blocks + b
             back_copy(layer, b, 1 - core).wait_recv()
@@ -503,6 +563,11 @@
             @pl.when(layer + 1 == layers)
             def _():
                 out_ref[block_rows(b), :] = states[state_rows(layers, b), :]
+
+        return tuple(
+            advance(at, s >= offset) for at, offset in zip(streams, offsets, strict=True))
+
+    lax.fori_loop(0, plan.steps, step, tuple((jnp.int32(0),) * 3 for _ in offsets))
 
     def all_sent(buf, count, sem):
         sent = buf.at[pl.ds(0, count)]
@@ -525,6 +590,11 @@
         @pl.when(p > 0)
         def _():
             all_sent(hid.at[d], plan.hids[d], hid_send.at[d])
+
+        @pl.when(p == n - 1)
+        def _():
+            for o in range(1, n):
+                all_sent(hid.at[d], plan.lasts[d], hid_send.at[d])
 
 
 def run(plan, *operands):
@@ -535,7 +605,7 @@
     n, nx, dl, nch, span, stages = plan.n, plan.nx, plan.dl, plan.nch, plan.span, plan.stages
     return pl.pallas_call(
         functools.partial(body_kernel, plan),
-        out_shape=jax.ShapeDtypeStruct((plan.tokens, dl), bf16),
+        out_shape=pltpu.VMEM((plan.tokens, dl), bf16),
         in_specs=[hbm] + [vmem] * 6 + [hbm] * 3,
         out_specs=vmem,
         scratch_shapes=[
@@ -561,19 +631,20 @@
             dma((2,)),
             dma((plan.layers,)),
             dma((2,)),
-            dma((2, stages, span)),
+            dma((2, plan.ring * span)),
             dma((2,)),
-            dma((2, stages, span)),
+            dma((2, plan.ring * span)),
+            dma((2, LAST)),
             dma((1,)),
-            dma((stages, n)),
+            dma((plan.blocks, n)),
             dma((1,)),
-            dma((stages, n)),
+            dma((plan.blocks, n)),
             dma((1,)),
-            dma((stages, nx)),
-            dma((stages,)),
-            dma((stages,)),
+            dma((2, nx)),
+            dma((2,)),
+            dma((2,)),
             dma((1,)),
-            dma((stages,)),
+            dma((2,)),
         ],
         compiler_params=pltpu.CompilerParams(
             collective_id=0, has_side_effects=True, vmem_limit_bytes=58 * 1024 * 1024

time: 228 us -> 221 us (0.969)
  Pallas kernels: 225 us -> 220 us
    pallas_call x1, Pallas kernels: 225 us -> 220 us  [run(): pl.pallas_call(functools.partial(body_kernel, plan), out_shape=pltpu.VMEM...]
where the time goes in v3:
time: 221 us
  Pallas kernels  220 us (100%)
    pallas_call x1, Pallas kernels, run(): pl.pallas_call(functools.partial(body_kernel, plan), out_shape=pltpu.VMEM...  220 us

profile of v3, /device:TPU:1, one launch (start us, length us, event | category | flops | bytes accessed | tf_op | source)
XLA Modules:
  0.0 220.9 jit_solution(7188701864620205385)
XLA Ops:
  0.0 220.0 %sublayers.1 = bf16[512,1024]{1,0:T(8,128)(2,1)S(1)} custom-call(bf16[512,1024]{1,0:T(8,128)(2,1)} %state_hbm.1, bf16[2,1024]{1,0:T(2,128)(2,1)} %pre_ref.1, bf16[2,1024]{1,0:T(2,128)(2,1)} %post_ref.1, bf16[3,2,2752]{2,1,0:T(2,128)(2,1)} %bitcast.6, bf16[3,2,2752]{2,1,0:T(2,128)(2,1)} %bitcast.7, bf16[2,2752]{1,0:T(2,128)(2,1)} %gb_ref.1, ...), custom_call_target="tpu_custom_call" | custom-call | tf_op jit(solution)/shard_map/sublayers/pallas_call | solution.py:606
  220.0 1.0 copy.12

commit v4 on v3

--- a/solution.py
+++ b/solution.py
@@ -11,9 +11,8 @@
 LANES = 128
 BLOCK = 128
 HALO = 8
-SUM_SKEW = 3
-HID_SKEW = 3
-LAST = 3
+HOP = 5
+LAST = 4
 
 epsilon = 1e-06
 residual_scale = 0.5
@@ -41,16 +40,20 @@
         self.hids = [
             layers * sum(len(self.chunks(d, b)) for b in range(self.blocks)) - self.lasts[d]
             for d in range(2)]
-        self.turn = (n - 1) * SUM_SKEW
-        self.done = self.turn + (n - 1) * HID_SKEW
-        self.pair_at = self.done + 2
-        self.x_at = self.pair_at + 8
-        self.norm_at = self.x_at + 3
+        assert n % 2 == 0
+        self.turn = self.after(n - 1)
+        self.done = self.after(2 * (n - 1))
+        self.pair_at = self.done + 1
+        self.x_at = self.pair_at + 5
+        self.norm_at = self.x_at + 6
         self.next_at = self.norm_at + 1
         least = max(self.span + self.next_at + 1, (self.blocks - 1) * self.span + self.turn + 2)
         self.lap = max(self.blocks, -(-least // self.span))
         self.steps = ((layers - 1) * self.lap + self.blocks) * self.span + self.next_at + 1
-        self.ring = -(-(SUM_SKEW + HID_SKEW + 2) // self.span)
+        self.ring = -(-(HOP + 4) // self.span)
+
+    def after(self, hops):
+        return hops * HOP // 2
 
     def chunks(self, d, b):
         return range((d + b // self.per_seq) % 2, self.nch, 2)
@@ -361,9 +364,13 @@
             device_id={"cb": peer}, device_id_type=MESH)
 
     offsets = [plan.turn, plan.done]
-    for d in range(2):
-        p = place(d)[0]
-        offsets += [p * SUM_SKEW, plan.done - p * HID_SKEW]
+    halves = []
+    for i in range(2):
+        d = (z + 1 + i) % 2
+        ahead = 2 * d - 1
+        p = jnp.where(d == 1, z, n - 1 - z)
+        halves.append((d, p, z + ahead, z - ahead))
+        offsets += [plan.after(p), plan.after(2 * (n - 1) - p)]
 
     def step(s, streams):
         turn_at, done_at = streams[0], streams[1]
@@ -393,10 +400,9 @@
             scale[block_rows(b), :] = scale_of(pre_sq, t, BLOCK)
             acc[block_rows(b), :] = jnp.zeros((BLOCK, dl), f32)
 
-        for d in range(2):
-            p, nxt, prv = place(d)
-            layer, b, j = sum_at[d]
-            live = live_at(sum_at[d], p * SUM_SKEW, s)
+        for i, (d, p, nxt, prv) in enumerate(halves):
+            layer, b, j = sum_at[i]
+            live = live_at(sum_at[i], plan.after(p), s)
             c = chunk_of(d, b, j)
             t = layer * blocks + b
 
@@ -418,8 +424,8 @@
 
                 @pl.when(p == 0)
                 def _():
-                    for i in range(2):
-                        part[d, part_tile(t, j, i)] = mine(i).astype(part.dtype)
+                    for side_at in range(2):
+                        part[d, part_tile(t, j, side_at)] = mine(side_at).astype(part.dtype)
                     part_do(d, t, j, c, nxt, start)
 
                 @pl.when((p > 0) & (p < n - 1))
@@ -441,12 +447,12 @@
                     first = one_of(b, range(0, blocks, plan.per_seq))
                     last = plan.packed & (c == nfull)
                     sides = []
-                    for i in range(2):
-                        arrived = jnp.where(last, 0.0, tile(i)) if i and plan.packed else tile(i)
-                        total = (arrived + mine(i)) * scale[block_rows(b), :]
-                        before = jnp.where(first, 0.0, halo[d, j, i])
-                        halo[d, j, i] = total[BLOCK - HALO :, :]
-                        at = i * side
+                    for k2 in range(2):
+                        arrived = jnp.where(last, 0.0, tile(k2)) if k2 and plan.packed else tile(k2)
+                        total = (arrived + mine(k2)) * scale[block_rows(b), :]
+                        before = jnp.where(first, 0.0, halo[d, j, k2])
+                        halo[d, j, k2] = total[BLOCK - HALO :, :]
+                        at = k2 * side
                         sides.append(conv(total, before, row[at : at + taps], row[at + taps]))
                     gate, up = sides
                     if plan.packed:
@@ -470,10 +476,8 @@
                 def _():
                     w_do(layer + 1, c, start)
 
-        for d in range(2):
-            p, nxt, prv = place(d)
-            layer, b, j = hid_at[d]
-            live = live_at(hid_at[d], plan.done - p * HID_SKEW, s)
+            layer, b, j = hid_at[i]
+            live = live_at(hid_at[i], plan.after(2 * (n - 1) - p), s)
             c = chunk_of(d, b, j)
             t = layer * blocks + b
 
@@ -491,10 +495,8 @@
                 def _():
                     last_copy(d, t, j, nxt).wait_recv()
 
-        for d in range(2):
-            p, nxt, prv = place(d)
-            layer, b, j = hid_at[d]
-            live = live_at(hid_at[d], plan.done - p * HID_SKEW, s)
+            layer, b, j = hid_at[i]
+            live = live_at(hid_at[i], plan.after(2 * (n - 1) - p), s)
             c = chunk_of(d, b, j)
 
             @pl.when(live & (c < nch))

time: 221 us -> 220 us (level)
  no operation moved by 1% of the time
where the time goes in v4:
time: 220 us
  Pallas kernels  219 us (100%)
    pallas_call x1, Pallas kernels, run(): pl.pallas_call(functools.partial(body_kernel, plan), out_shape=pltpu.VMEM...  219 us

profile of v4, /device:TPU:1, one launch (start us, length us, event | category | flops | bytes accessed | tf_op | source)
XLA Modules:
  0.0 219.9 jit_solution(16457353298087928651)
XLA Ops:
  0.0 218.9 %sublayers.1 = bf16[512,1024]{1,0:T(8,128)(2,1)S(1)} custom-call(bf16[512,1024]{1,0:T(8,128)(2,1)} %state_hbm.1, bf16[2,1024]{1,0:T(2,128)(2,1)} %pre_ref.1, bf16[2,1024]{1,0:T(2,128)(2,1)} %post_ref.1, bf16[3,2,2752]{2,1,0:T(2,128)(2,1)} %bitcast.6, bf16[3,2,2752]{2,1,0:T(2,128)(2,1)} %bitcast.7, bf16[2,2752]{1,0:T(2,128)(2,1)} %gb_ref.1, ...), custom_call_target="tpu_custom_call" | custom-call | tf_op jit(solution)/shard_map/sublayers/pallas_call | solution.py:608
  218.9 1.0 copy.12
